TPU v7x, 32 devices: a whole 2x2x4 slice. The times are simulated.
32 devices in a mesh: sp: 8 (over z, x), tp: 4 (over y, core).
Axes of the slice: x: 2, y: 2, z: 4, core: 2. Of those that a mesh axis runs over, the one named last changes fastest.
Arguments:
- resid: bfloat16 [1024, 2048], P('sp'), may hold values from -8 to 8
- a_val: bfloat16 [1024, 1024], P('sp', 'tp'), may hold values from -8 to 8
- a_gate: bfloat16 [1024, 1024], P('sp', 'tp'), may hold values from -6 to 6
- conv_kernel: bfloat16 [31, 1024], P(None, 'tp'), may hold values from -1 to 1
- conv_bias: float32 [1024], P('tp'), may hold values from -3 to 3
- ln_gain: float32 [1024], P('tp'), may hold values from 0.1 to 1.9
- ln_bias: float32 [1024], P('tp'), may hold values from -3 to 3
- w_out: bfloat16 [1024, 2048], P('tp'), may hold values from -0.1875 to 0.1875
- ffn_gain: float32 [2048], replicated, may hold values from 0.1 to 1.9
- routes: int32 [1024, 4], P('sp'), may hold values from 0 to 7, all different within a row; in each aligned block of 128 rows (0 to 127, 128 to 255, ...) at most 128 rows name the same one
- route_weights: float32 [1024, 4], P('sp'), may hold values from 0.15 to 1.2
- exp_gate: bfloat16 [8, 2048, 4096], P('sp', None, 'tp'), may hold values from -0.125 to 0.125
- exp_up: bfloat16 [8, 2048, 4096], P('sp', None, 'tp'), may hold values from -0.125 to 0.125
- exp_down: bfloat16 [8, 4096, 2048], P('sp', None, 'tp'), may hold values from -0.09375 to 0.09375
- sh_gate: bfloat16 [2048, 512], P(None, 'tp'), may hold values from -0.125 to 0.125
- sh_up: bfloat16 [2048, 512], P(None, 'tp'), may hold values from -0.125 to 0.125
- sh_down: bfloat16 [512, 2048], P(None, 'tp'), may hold values from -0.25 to 0.25
Outputs:
- result: bfloat16 [1024, 2048], P('sp', 'tp')
Inputs may be any that keep to these rules, and one draw needn't show every extreme that they name: `routes`: among the 128 rows of one index of sp, each expert is named at most 128 times, a bound that some block reaches; a row names 4 different experts.
All inputs are finite; a program needn't handle non-finite values.
Results may differ from a plain program's by a relative error of at most 0.007.
Values may be sent and summed in bfloat16 or wider, within the bound.
A program may use at most 64 MiB of HBM per device.

v0:
```python
import jax
import jax.numpy as jnp
from jax import lax
from jax.sharding import PartitionSpec as P

LN_EPS = 1e-05
RMS_EPS = 1e-06


def shifted(value, axis, by):
    size = lax.axis_size(axis)
    pairs = [(i, i + by) for i in range(size) if 0 <= i + by < size]
    return lax.ppermute(value, axis, pairs)


def body_slots(
    resid,
    a_val,
    a_gate,
    conv_kernel,
    conv_bias,
    ln_gain,
    ln_bias,
    w_out,
    ffn_gain,
    routes,
    route_weights,
    exp_gate,
    exp_up,
    exp_down,
    sh_gate,
    sh_up,
    sh_down,
):
    tp_count = lax.axis_size("tp")
    tp_place = lax.axis_index("tp")
    sp_count = lax.axis_size("sp")
    tok_rows = resid.shape[0]
    model_width = resid.shape[1]
    col_width = model_width // tp_count
    col_start = tp_place * col_width
    conv_span = conv_kernel.shape[0]
    channels_all = a_val.shape[1] * tp_count
    gated_in = (a_val.astype(jnp.float32) * jax.nn.sigmoid(a_gate.astype(jnp.float32))).astype(
        jnp.bfloat16
    )
    before = shifted(gated_in[tok_rows - (conv_span - 1) :], "sp", 1)
    padded = jnp.concatenate([before, gated_in], axis=0).astype(jnp.float32)
    kernel = conv_kernel.astype(jnp.float32)

    def add_tap(offset, running):
        window_rows = lax.dynamic_slice_in_dim(padded, offset, tok_rows, 0)
        return running + lax.dynamic_slice_in_dim(kernel, offset, 1, 0) * window_rows

    start_sum = jnp.broadcast_to(conv_bias[None, :], gated_in.shape)
    conv_out = lax.fori_loop(0, conv_span, add_tap, start_sum)
    row_sums = lax.psum((jnp.sum(conv_out, axis=1), jnp.sum(conv_out * conv_out, axis=1)), "tp")
    channel_mean = row_sums[0] / channels_all
    channel_var = row_sums[1] / channels_all - channel_mean * channel_mean
    scaled = (conv_out - channel_mean[:, None]) * lax.rsqrt(
        channel_var[:, None] + LN_EPS
    ) * ln_gain[None, :] + ln_bias[None, :]
    mixed_out = jax.nn.silu(scaled).astype(jnp.bfloat16)
    partial_proj = jnp.dot(mixed_out, w_out, preferred_element_type=jnp.float32)
    projected = lax.psum(partial_proj, "tp")
    middle = (resid.astype(jnp.float32) + projected).astype(jnp.bfloat16)
    middle_f = middle.astype(jnp.float32)
    inverse = lax.rsqrt(jnp.mean(middle_f * middle_f, axis=1, keepdims=True) + RMS_EPS)
    normed = (middle_f * inverse * ffn_gain[None, :]).astype(jnp.bfloat16)
    middle_cols = lax.dynamic_slice_in_dim(middle, col_start, col_width, 1)
    shared_gate = jnp.dot(normed, sh_gate, preferred_element_type=jnp.float32)
    shared_up = jnp.dot(normed, sh_up, preferred_element_type=jnp.float32)
    shared_hidden = (jax.nn.silu(shared_gate) * shared_up).astype(jnp.bfloat16)
    weight_rows = sh_down
    shared = jnp.dot(
        lax.all_gather(shared_hidden, "tp", axis=1, tiled=True),
        weight_rows,
        preferred_element_type=jnp.float32,
    )
    top_count = routes.shape[1]
    local_experts = exp_gate.shape[0]
    experts_all = local_experts * sp_count
    capacity = max(2 * tok_rows * top_count // experts_all, tp_count)
    pair_count = tok_rows * top_count
    chosen = routes.reshape(pair_count)
    one_hot = (chosen[:, None] == jnp.arange(experts_all, dtype=jnp.int32)[None, :]).astype(
        jnp.int32
    )
    earlier = jnp.cumsum(one_hot, axis=0) - one_hot
    place_in = jnp.sum(earlier * one_hot, axis=1)
    slot_of = chosen * capacity + place_in
    owner_ids = (
        jnp.zeros((experts_all * capacity,), jnp.int32)
        .at[slot_of]
        .set(jnp.arange(pair_count, dtype=jnp.int32) + 1)
    )
    owner_grid = owner_ids.reshape(sp_count, local_experts, capacity)
    part_slots = capacity // tp_count
    own_owners = lax.dynamic_slice_in_dim(owner_grid, tp_place * part_slots, part_slots, 2)
    source_row = jnp.maximum(own_owners - 1, 0) // top_count
    taken = normed[source_row.reshape(-1)].reshape(own_owners.shape + (model_width,))
    landed = lax.all_to_all(
        jnp.where((own_owners > 0)[..., None], taken, jnp.zeros((), jnp.bfloat16)),
        "sp",
        split_axis=0,
        concat_axis=0,
        tiled=True,
    )
    arrived = lax.all_gather(landed, "tp", axis=2, tiled=True)
    gate_part = jnp.einsum("sxcd,xdf->sxcf", arrived, exp_gate, preferred_element_type=jnp.float32)
    up_part = jnp.einsum("sxcd,xdf->sxcf", arrived, exp_up, preferred_element_type=jnp.float32)
    expert_hidden = (jax.nn.silu(gate_part) * up_part).astype(jnp.bfloat16)
    weight_rows = exp_down
    expert_sum = jnp.einsum(
        "sxcf,xfd->sxcd",
        lax.all_gather(expert_hidden, "tp", axis=3, tiled=True),
        weight_rows,
        preferred_element_type=jnp.float32,
    )
    expert_out = expert_sum.astype(jnp.bfloat16)
    returned = lax.all_to_all(expert_out, "sp", split_axis=0, concat_axis=0, tiled=True)
    flat_out = returned.reshape(experts_all * capacity, col_width)
    picked = flat_out[slot_of].astype(jnp.float32).reshape(tok_rows, top_count, col_width)
    routed = jnp.sum(picked * route_weights[:, :, None], axis=1)
    return (middle_cols.astype(jnp.float32) + shared + routed).astype(jnp.bfloat16)


def swapped(value, axis, bit):
    size = lax.axis_size(axis)
    return lax.ppermute(value, axis, [(i, i ^ bit) for i in range(size)])


def body_dense(
    resid,
    a_val,
    a_gate,
    conv_kernel,
    conv_bias,
    ln_gain,
    ln_bias,
    w_out,
    ffn_gain,
    routes,
    route_weights,
    exp_gate,
    exp_up,
    exp_down,
    sh_gate,
    sh_up,
    sh_down,
):
    tp_count = lax.axis_size("tp")
    tp_place = lax.axis_index("tp")
    core = tp_place % 2
    row = tp_place // 2
    sp_count = lax.axis_size("sp")
    tok_rows, model_width = resid.shape
    col_width = model_width // tp_count
    half_width = model_width // 2
    part_hidden = exp_gate.shape[2]
    conv_span = conv_kernel.shape[0]
    channels_all = a_val.shape[1] * tp_count
    other_rows = lax.dynamic_slice_in_dim(
        exp_down[0], (1 - row) * 2 * part_hidden, 2 * part_hidden, 0
    )
    swapped_down = swapped(other_rows, "tp", 2)
    gated_in = (a_val.astype(jnp.float32) * jax.nn.sigmoid(a_gate.astype(jnp.float32))).astype(
        jnp.bfloat16
    )
    before = shifted(gated_in[tok_rows - (conv_span - 1) :], "sp", 1)
    expert_ids = jnp.arange(sp_count, dtype=jnp.int32)
    weight_mat = jnp.sum(
        jnp.where(routes[:, :, None] == expert_ids[None, None, :], route_weights[:, :, None], 0.0),
        axis=1,
    )
    weight_all = lax.all_gather(weight_mat, "sp", axis=0, tiled=True)
    weight_own = lax.dynamic_slice_in_dim(weight_all, lax.axis_index("sp"), 1, 1)
    padded = jnp.concatenate([before, gated_in], axis=0).astype(jnp.float32)
    kernel = conv_kernel.astype(jnp.float32)
    conv_out = jnp.broadcast_to(conv_bias[None, :], gated_in.shape)
    for tap in range(conv_span):
        conv_out = conv_out + kernel[tap : tap + 1] * padded[tap : tap + tok_rows]
    row_sums = lax.psum((jnp.sum(conv_out, axis=1), jnp.sum(conv_out * conv_out, axis=1)), "tp")
    channel_mean = row_sums[0] / channels_all
    channel_var = row_sums[1] / channels_all - channel_mean * channel_mean
    scaled = (conv_out - channel_mean[:, None]) * lax.rsqrt(
        channel_var[:, None] + LN_EPS
    ) * ln_gain[None, :] + ln_bias[None, :]
    mixed_out = jax.nn.silu(scaled).astype(jnp.bfloat16)
    partial_proj = jnp.dot(mixed_out, w_out, preferred_element_type=jnp.float32)
    give = lax.dynamic_slice_in_dim(partial_proj, (1 - core) * half_width, half_width, 1)
    keep = lax.dynamic_slice_in_dim(partial_proj, core * half_width, half_width, 1)
    chip_sum = keep + swapped(give.astype(jnp.bfloat16), "tp", 1).astype(jnp.float32)
    chip_sum = chip_sum.astype(jnp.bfloat16)
    half_sum = chip_sum.astype(jnp.float32) + swapped(chip_sum, "tp", 2).astype(jnp.float32)
    resid_half = lax.dynamic_slice_in_dim(resid, core * half_width, half_width, 1)
    mid_half = (resid_half.astype(jnp.float32) + half_sum).astype(jnp.bfloat16)
    mid_all = lax.all_gather(mid_half, "sp", axis=0, tiled=True)
    mid_peer = swapped(mid_half, "tp", 1)
    first = jnp.where(core == 0, mid_half, mid_peer)
    second = jnp.where(core == 0, mid_peer, mid_half)
    middle = jnp.concatenate([first, second], axis=1)
    middle_f = middle.astype(jnp.float32)
    inverse = lax.rsqrt(jnp.mean(middle_f * middle_f, axis=1, keepdims=True) + RMS_EPS)
    normed = (middle_f * inverse * ffn_gain[None, :]).astype(jnp.bfloat16)
    middle_cols = lax.dynamic_slice_in_dim(middle, tp_place * col_width, col_width, 1)
    shared_gate = jnp.dot(normed, sh_gate, preferred_element_type=jnp.float32)
    shared_up = jnp.dot(normed, sh_up, preferred_element_type=jnp.float32)
    shared_hidden = (jax.nn.silu(shared_gate) * shared_up).astype(jnp.bfloat16)
    shared = jnp.dot(
        lax.all_gather(shared_hidden, "tp", axis=1, tiled=True),
        sh_down,
        preferred_element_type=jnp.float32,
    )
    mid_all_peer = swapped(mid_all, "tp", 1)
    rows_first = jnp.where(core == 0, mid_all, mid_all_peer)
    rows_second = jnp.where(core == 0, mid_all_peer, mid_all)
    rows_f = jnp.concatenate([rows_first, rows_second], axis=1).astype(jnp.float32)
    rows_inverse = lax.rsqrt(jnp.mean(rows_f * rows_f, axis=1, keepdims=True) + RMS_EPS)
    rows = (rows_f * rows_inverse * ffn_gain[None, :]).astype(jnp.bfloat16)
    gate_part = jnp.dot(rows, exp_gate[0], preferred_element_type=jnp.float32)
    up_part = jnp.dot(rows, exp_up[0], preferred_element_type=jnp.float32)
    hidden = (jax.nn.silu(gate_part) * up_part).astype(jnp.bfloat16)
    hidden_peer = swapped(hidden, "tp", 1)
    own_at = tp_place * part_hidden
    peer_at = (tp_place ^ 1) * part_hidden
    stay = lax.dynamic_slice_in_dim
    out_own = jnp.dot(
        hidden, stay(exp_down[0], own_at, part_hidden, 0), preferred_element_type=jnp.float32
    ) + jnp.dot(
        hidden_peer, stay(exp_down[0], peer_at, part_hidden, 0), preferred_element_type=jnp.float32
    )
    out_far = jnp.dot(
        hidden,
        stay(swapped_down, core * part_hidden, part_hidden, 0),
        preferred_element_type=jnp.float32,
    ) + jnp.dot(
        hidden_peer,
        stay(swapped_down, (1 - core) * part_hidden, part_hidden, 0),
        preferred_element_type=jnp.float32,
    )
    both = jnp.concatenate([out_own * weight_own, out_far * weight_own], axis=1).astype(
        jnp.bfloat16
    )
    summed = lax.psum_scatter(both, "sp", scatter_dimension=0, tiled=True)
    far = swapped(summed[:, col_width:], "tp", 2)
    routed = summed[:, :col_width].astype(jnp.float32) + far.astype(jnp.float32)
    return (middle_cols.astype(jnp.float32) + shared + routed).astype(jnp.bfloat16)


def body(*args):
    tok_rows = args[0].shape[0]
    top_count = args[9].shape[1]
    local_experts = args[11].shape[0]
    experts_all = local_experts * lax.axis_size("sp")
    capacity = 2 * tok_rows * top_count // experts_all
    if local_experts == 1 and lax.axis_size("tp") == 4 and (capacity >= tok_rows):
        return body_dense(*args)
    return body_slots(*args)


def solution(mesh):
    in_specs = (
        P("sp", None),
        P("sp", "tp"),
        P("sp", "tp"),
        P(None, "tp"),
        P("tp"),
        P("tp"),
        P("tp"),
        P("tp", None),
        P(),
        P("sp", None),
        P("sp", None),
        P("sp", None, "tp"),
        P("sp", None, "tp"),
        P("sp", None, "tp"),
        P(None, "tp"),
        P(None, "tp"),
        P(None, "tp"),
    )
    out_specs = P("sp", "tp")
    return jax.shard_map(body, mesh=mesh, in_specs=in_specs, out_specs=out_specs, check_vma=False)
```

profile of v0, /device:TPU:0, one launch (start us, length us, event | category | flops | bytes accessed | tf_op | source)
XLA Modules:
  0.0 230.6 jit_solution(7663626764208417222)
XLA Ops:
  6.5 1.0 multiply_convert_fusion.4
  7.6 4.9 %collective-permute-start = (bf16[30,256]{1,0:T(8,128)(2,1)S(1)}, bf16[30,256]{1,0:T(8,128)(2,1)S(1)}, u32[]{:S(2)}, u32[]{:S(2)}) collective-permute-start(bf16[30,256]{1,0:T(8,128)(2,1)S(1)} %slice.261), channel_id=1, source_target_pairs={{0,4},{4,8},{8,12},{12,16},{16,20},{20,24},{24,28},{1,5},{5,9},{9,... | collective-permute-start | bytes 46088 | tf_op jit(solution)/shard_map/ppermute | solution.py:13
  12.4 1.0 fusion.73
  13.5 1.0 fusion.74
  14.5 1.3 fusion.71
  15.8 6.3 %all-reduce = (f32[128]{0:T(128)S(1)}, f32[128]{0:T(128)S(1)}) all-reduce(f32[128]{0:T(128)S(1)} %get-tuple-element.6, f32[128]{0:T(128)S(1)} %get-tuple-element.5), channel_id=1, replica_groups=mesh['sp'=8,'tp'=4] {'tp'}, use_global_device_ids=true, to_apply=%region_3.4 | all-reduce | flops 256 | bytes 2048 | tf_op jit(solution)/shard_map/psum | solution.py:183
  22.2 0.4 fusion.51
  22.6 0.1 collective-permute-start.1
  22.7 1.5 collective-permute-done.1
  24.2 0.1 add_convert_fusion.1
  24.3 1.1 collective-permute-start.2
  25.4 7.3 %collective-permute-done.2 = bf16[128,1024]{1,0:T(8,128)(2,1)S(1)} collective-permute-done((bf16[128,1024]{1,0:T(8,128)(2,1)S(1)}, bf16[128,1024]{1,0:T(8,128)(2,1)S(1)}, u32[]{:S(2)}, u32[]{:S(2)}) %collective-permute-start.2) | collective-permute-done | bytes 262176 | tf_op jit(solution)/shard_map/ppermute | solution.py:130
  32.7 0.8 add_convert_fusion
  33.5 0.0 all-gather.2.cloned.1.call-update
  33.6 0.0 reduce-scatter.2.cloned.1.call-start
  33.6 50.1 %all-gather.2.cloned.1.call-done = bf16[1024,1024]{1,0:T(8,128)(2,1)} async-done(((bf16[128,1024]{1,0:T(8,128)(2,1)}), bf16[1024,1024]{1,0:T(8,128)(2,1)}) %all-gather.2.cloned.1.call-update) | async-done | bytes 2097168 | tf_op jit(solution)/shard_map/all_gather | solution.py:198
  83.8 1.7 dynamic-slice_bitcast_fusion
  85.5 1.5 collective-permute-start.6
  87.0 1.2 collective-permute-done.4
  88.3 2.5 %broadcast_select_fusion.1 = (bf16[1024,1024]{1,0:T(8,128)(2,1)S(1)}, bf16[1024,1024]{1,0:T(8,128)(2,1)S(1)}) fusion(bf16[1024,1024]{1,0:T(8,128)(2,1)} %all-gather.2.cloned.1.call-done, bf16[1024,1024]{1,0:T(8,128)(2,1)} %collective-permute-done.4, pred[]{:T(512)S(6)} %eq.10), kind=kLoop, calls=%fused_computation.16 | loop fusion | flops 2097152 | bytes 8388609 | tf_op jit(solution)/shard_map/jit(_where)/select_n | solution.py:216
  90.8 0.0 copy-start.8
  90.8 1.0 fusion
  91.8 1.2 copy-done.8
  92.9 4.6 %fusion.5 = f32[1024,1024]{1,0:T(8,128)S(1)} fusion(bf16[1,2048,1024]{2,1,0:T(8,128)(2,1)S(1)} %copy-done.8, f32[2048]{0:T(1024)S(1)} %copy-done.11, f32[1024]{0:T(1024)S(1)} %add_rsqrt_fusion, bf16[1024,1024]{1,0:T(8,128)(2,1)S(1)} %get-tuple-element.11, bf16[1024,1024]{1,0:T(8,128)(2,1)S(1)} %get-tuple-element.10), kind=kOutput, calls=%fused_computation.8 | convolution fusion | flops 4309647360 | bytes 12595200 | tf_op jit(solution)/shard_map/dot_general | solution.py:221
  97.5 0.0 copy-start.4
  97.5 0.0 copy-start.5
  97.5 6.4 %multiply_convert_fusion = bf16[1024,1024]{1,0:T(8,128)(2,1)} fusion(f32[1024,1024]{1,0:T(8,128)S(1)} %fusion.5, bf16[1,2048,1024]{2,1,0:T(8,128)(2,1)S(1)} %copy-done.9, f32[2048]{0:T(1024)S(1)} %copy-done.11, f32[1024]{0:T(1024)S(1)} %add_rsqrt_fusion, bf16[1024,1024]{1,0:T(8,128)(2,1)S(1)} %get-tuple-element.11, bf16[1024,1024]{1,0:T(8,128)(2,1)S(1)} %get-tuple-element.10), kind=kOutput, calls=%fused_computation.10 | convolution fusion | flops 4315938816 | bytes 14692352 | tf_op jit(solution)/shard_map/dot_general | solution.py:222
  103.9 0.1 collective-permute-start.5
  104.1 30.8 %all_gather.11 = f32[1024,8]{0,1:T(8,128)S(1)} all-gather(f32[128,8]{0,1:T(8,128)S(1)} %select_reduce_fusion), channel_id=1, replica_groups=mesh['sp'=8,'tp'=4] {'sp'}, dimensions={0}, use_global_device_ids=true | all-gather | bytes 36864 | tf_op jit(solution)/shard_map/all_gather | solution.py:176
  134.9 3.1 %fusion.12 = f32[1024,512]{1,0:T(8,128)S(1)} fusion(bf16[1024,1024]{1,0:T(8,128)(2,1)} %multiply_convert_fusion, bf16[1,4096,512]{2,1,0:T(8,128)(2,1)} %param.30, s32[]{:T(128)S(6)} %select_n.73), kind=kOutput, calls=%fused_computation.25 | convolution fusion | flops 1073741824 | bytes 5242884 | tf_op jit(solution)/shard_map/dot_general | solution.py:228
  138.0 3.1 %fusion.14 = f32[1024,512]{1,0:T(8,128)S(1)} fusion(bf16[1024,1024]{1,0:T(8,128)(2,1)} %collective-permute-done.5, bf16[2048,512]{1,0:T(8,128)(2,1)} %collective-permute-done.6, s32[]{:T(128)S(6)} %select_n.66), kind=kOutput, calls=%fused_computation.27 | convolution fusion | flops 1073741824 | bytes 5242884 | tf_op jit(solution)/shard_map/dot_general | solution.py:237
  141.1 3.1 %multiply_convert_fusion.1 = bf16[1024,512]{1,0:T(8,128)(2,1)S(1)} fusion(f32[1024,512]{1,0:T(8,128)S(1)} %fusion.14, bf16[1024,1024]{1,0:T(8,128)(2,1)} %multiply_convert_fusion, bf16[2048,512]{1,0:T(8,128)(2,1)} %collective-permute-done.6, s32[]{:T(128)S(6)} %select_n.65, f32[1024]{0:T(1024)S(1)} %bitcast.88), kind=kOutput, calls=%fused_computation.12 | convolution fusion | flops 1075314688 | bytes 6295556 | tf_op jit(solution)/shard_map/dot_general | solution.py:233
  144.2 3.1 %multiply_convert_fusion.2 = bf16[1024,512]{1,0:T(8,128)(2,1)S(1)} fusion(f32[1024,512]{1,0:T(8,128)S(1)} %fusion.12, bf16[1024,1024]{1,0:T(8,128)(2,1)} %collective-permute-done.5, f32[1024]{0:T(1024)S(1)} %bitcast.89, bf16[1,4096,512]{2,1,0:T(8,128)(2,1)} %param.30, s32[]{:T(128)S(6)} %select_n.74), kind=kOutput, calls=%fused_computation.14 | convolution fusion | flops 1075314688 | bytes 6295556 | tf_op jit(solution)/shard_map/dot_general | solution.py:230
  147.4 0.0 copy-start.10
  147.4 1.6 pad_maximum_fusion.1
  149.0 0.0 reduce-scatter.2.cloned.1.call-update
  149.0 0.1 collective-permute-start.3
  149.1 1.5 collective-permute-done.3
  150.7 0.2 fusion.8
  150.9 0.4 fusion.63
  151.2 1.4 fusion.7
  152.6 5.4 %all_gather.9 = bf16[128,512]{1,0:T(8,128)(2,1)S(1)} all-gather(bf16[128,128]{1,0:T(8,128)(2,1)S(1)} %fusion.7), channel_id=1, replica_groups=mesh['sp'=8,'tp'=4] {'tp'}, dimensions={1}, use_global_device_ids=true | all-gather | bytes 163840 | tf_op jit(solution)/shard_map/all_gather | solution.py:211
  158.1 58.0 %reduce-scatter.2.cloned.1.call-done = bf16[128,1024]{1,0:T(8,128)(2,1)} async-done(((bf16[1024,1024]{1,0:T(8,128)(2,1)}), bf16[128,1024]{1,0:T(8,128)(2,1)}) %reduce-scatter.2.cloned.1.call-update) | async-done | bytes 262160 | tf_op jit(solution)/shard_map/reduce_scatter | solution.py:245
  216.1 0.9 slice.324
  217.0 1.5 collective-permute-start.7
  218.5 0.2 fusion.75
  218.8 3.3 %collective-permute-done.7 = bf16[128,512]{1,0:T(8,128)(2,1)S(1)} collective-permute-done((bf16[128,512]{1,0:T(8,128)(2,1)S(1)}, bf16[128,512]{1,0:T(8,128)(2,1)S(1)}, u32[]{:S(2)}, u32[]{:S(2)}) %collective-permute-start.7) | collective-permute-done | bytes 131104 | tf_op jit(solution)/shard_map/ppermute | solution.py:130
  222.0 1.7 add_convert_fusion.2
  (33 shorter events, 0.2 us)
Async XLA Ops:
  6.5 15.6 %copy-start = (bf16[256,2048]{1,0:T(8,128)(2,1)S(1)}, bf16[256,2048]{1,0:T(8,128)(2,1)}, u32[]{:S(2)}) copy-start(bf16[256,2048]{1,0:T(8,128)(2,1)} %param.24) | copy-start | bytes 3145732
  6.5 15.6 %copy-start.6 = (f32[256]{0:T(256)S(1)}, f32[256]{0:T(256)}, u32[]{:S(2)}) copy-start(f32[256]{0:T(256)} %param.23) | copy-start | bytes 3076
  6.5 15.7 %copy-start.7 = (f32[256]{0:T(256)S(1)}, f32[256]{0:T(256)}, u32[]{:S(2)}) copy-start(f32[256]{0:T(256)} %param.22) | copy-start | bytes 3076
  6.5 77.2 %all-gather.2.cloned.1.call-start = ((), (), s32[]{:S(2)}) async-start(), calls=%async_computation.1 | async-start | bytes 2359296 | tf_op jit(solution)/shard_map/all_gather | solution.py:198
  7.6 6.9 %collective-permute-start = (bf16[30,256]{1,0:T(8,128)(2,1)S(1)}, bf16[30,256]{1,0:T(8,128)(2,1)S(1)}, u32[]{:S(2)}, u32[]{:S(2)}) collective-permute-start(bf16[30,256]{1,0:T(8,128)(2,1)S(1)} %slice.261), channel_id=1, source_target_pairs={{0,4},{4,8},{8,12},{12,16},{16,20},{20,24},{24,28},{1,5},{5,9},{9,... | collective-permute-start | bytes 46088 | tf_op jit(solution)/shard_map/ppermute | solution.py:13
  14.5 18.3 %copy-start.3 = (bf16[128,2048]{1,0:T(8,128)(2,1)S(1)}, bf16[128,2048]{1,0:T(8,128)(2,1)}, u32[]{:S(2)}) copy-start(bf16[128,2048]{1,0:T(8,128)(2,1)} %param.17) | copy-start | bytes 1572868
  22.6 1.6 collective-permute-start.1
  24.3 8.4 %collective-permute-start.2 = (bf16[128,1024]{1,0:T(8,128)(2,1)S(1)}, bf16[128,1024]{1,0:T(8,128)(2,1)S(1)}, u32[]{:S(2)}, u32[]{:S(2)}) collective-permute-start(bf16[128,1024]{1,0:T(8,128)(2,1)S(1)} %add_convert_fusion.1), channel_id=1, source_target_pairs={{0,2},{1,3},{2,0},{3,1},{4,6},{5,7},{6,4},{7,5},{8,10},{9,11},{10,... | collective-permute-start | bytes 786440 | tf_op jit(solution)/shard_map/ppermute | solution.py:130
  33.6 182.5 %reduce-scatter.2.cloned.1.call-start = ((), (), s32[]{:S(2)}) async-start(), calls=%async_computation.2 | async-start | bytes 2359296 | tf_op jit(solution)/shard_map/reduce_scatter | solution.py:245
  83.8 4.5 %collective-permute-start.4 = (bf16[1024,1024]{1,0:T(8,128)(2,1)}, bf16[1024,1024]{1,0:T(8,128)(2,1)}, u32[]{:S(2)}, u32[]{:S(2)}) collective-permute-start(bf16[1024,1024]{1,0:T(8,128)(2,1)} %all-gather.2.cloned.1.call-done), channel_id=1, source_target_pairs={{0,1},{1,0},{2,3},{3,2},{4,5},{5,4},{6,7},{7,6},{8,9},{9,8},{10,11... | collective-permute-start | bytes 6291464 | tf_op jit(solution)/shard_map/ppermute | solution.py:130
  85.5 52.5 %collective-permute-start.6 = (bf16[2048,512]{1,0:T(8,128)(2,1)S(1)}, bf16[2048,512]{1,0:T(8,128)(2,1)}, u32[]{:S(2)}, u32[]{:S(2)}) collective-permute-start(bf16[2048,512]{1,0:T(8,128)(2,1)S(1)} %dynamic-slice_bitcast_fusion), channel_id=1, source_target_pairs={{0,2},{1,3},{2,0},{3,1},{4,6},{5,7},{6,4},{7,5},{8,10},{9,11},{10,... | collective-permute-start | bytes 6291464 | tf_op jit(solution)/shard_map/ppermute | solution.py:130
  90.8 2.2 copy-start.8
  90.8 2.2 copy-start.11
  92.9 4.6 %copy-start.9 = (bf16[1,2048,1024]{2,1,0:T(8,128)(2,1)S(1)}, bf16[1,2048,1024]{2,1,0:T(8,128)(2,1)}, u32[]{:S(2)}) copy-start(bf16[1,2048,1024]{2,1,0:T(8,128)(2,1)} %param.29) | copy-start | bytes 12582916
  97.5 6.5 %copy-start.4 = (f32[128,4]{0,1:T(4,128)S(1)}, f32[128,4]{0,1:T(4,128)}, u32[]{:S(2)}) copy-start(f32[128,4]{0,1:T(4,128)} %param.27) | copy-start | bytes 6148
  97.5 6.5 %copy-start.5 = (s32[128,4]{0,1:T(4,128)S(1)}, s32[128,4]{0,1:T(4,128)}, u32[]{:S(2)}) copy-start(s32[128,4]{0,1:T(4,128)} %param.26) | copy-start | bytes 6148
  103.9 34.1 %collective-permute-start.5 = (bf16[1024,1024]{1,0:T(8,128)(2,1)}, bf16[1024,1024]{1,0:T(8,128)(2,1)}, u32[]{:S(2)}, u32[]{:S(2)}) collective-permute-start(bf16[1024,1024]{1,0:T(8,128)(2,1)} %multiply_convert_fusion), channel_id=1, source_target_pairs={{0,1},{1,0},{2,3},{3,2},{4,5},{5,4},{6,7},{7,6},{8,9},{9,8},{10,11... | collective-permute-start | bytes 6291464 | tf_op jit(solution)/shard_map/ppermute | solution.py:130
  147.4 1.6 copy-start.1
  147.4 3.5 %copy-start.10 = (bf16[2048,128]{1,0:T(8,128)(2,1)S(1)}, bf16[2048,128]{1,0:T(8,128)(2,1)}, u32[]{:S(2)}) copy-start(bf16[2048,128]{1,0:T(8,128)(2,1)} %param.31) | copy-start | bytes 1572868
  149.0 69.6 %copy-start.2 = (bf16[512,512]{1,0:T(8,128)(2,1)S(1)}, bf16[512,512]{1,0:T(8,128)(2,1)}, u32[]{:S(2)}) copy-start(bf16[512,512]{1,0:T(8,128)(2,1)} %param.33) | copy-start | bytes 1572868
  149.0 1.6 collective-permute-start.3
  217.0 5.0 %collective-permute-start.7 = (bf16[128,512]{1,0:T(8,128)(2,1)S(1)}, bf16[128,512]{1,0:T(8,128)(2,1)S(1)}, u32[]{:S(2)}, u32[]{:S(2)}) collective-permute-start(bf16[128,512]{1,0:T(8,128)(2,1)S(1)} %slice.324), channel_id=1, source_target_pairs={{0,2},{1,3},{2,0},{3,1},{4,6},{5,7},{6,4},{7,5},{8,10},{9,11},{10,... | collective-permute-start | bytes 393224 | tf_op jit(solution)/shard_map/ppermute | solution.py:130
Sparse Core Ops, SparseCore 0:
  33.7 50.0 all-gather.1
  149.1 66.9 reduce-scatter.1
where the time goes:
time: 231 us
  waiting for transfers between devices  123 us (53%)
  blocking collectives  42.6 us (18%)
  matrix products  25.8 us (11%)
  between operations  13.7 us (6%)
  other arithmetic  10.3 us (4%)
  starting transfers between devices  9.37 us (4%)
  local copies, waits for them, and re-layouts  5.9 us (3%)
    reduce_scatter x1, waiting for transfers between devices, body_dense(): summed = lax.psum_scatter(both, 'sp', scatter_dimension=0, tiled=True)  58 us
    all_gather x1, waiting for transfers between devices, body_dense(): mid_all = lax.all_gather(mid_half, 'sp', axis=0, tiled=True)  50.1 us
    all_gather x1, blocking collectives, body_dense(): weight_all = lax.all_gather(weight_mat, 'sp', axis=0, tiled=True)  30.8 us
    ppermute x7, waiting for transfers between devices, swapped(): return lax.ppermute(value, axis, [(i, i ^ bit) for i in range(size)])  14.8 us
    dot_general x1, matrix products, body_dense(): up_part = jnp.dot(rows, exp_up[0], preferred_element_type=jnp.float32)  6.37 us
    psum x1, blocking collectives, body_dense(): lax.psum((jnp.sum(conv_out, axis=1), jnp.sum(conv_out * conv_out, axis=1)...  6.33 us
    all_gather x1, blocking collectives, body_dense(): lax.all_gather(shared_hidden, 'tp', axis=1, tiled=True)  5.45 us
    ppermute x1, starting transfers between devices, shifted(): return lax.ppermute(value, axis, pairs)  4.87 us
  transfers between devices with their start and end apart: 10, of which 7 were waited for; matrix products, arithmetic and copies ran while one was open for 10% of the time, Pallas kernels for 0%

commit v1 on v0

--- a/solution.py
+++ b/solution.py
@@ -5,6 +5,21 @@
 
 LN_EPS = 1e-05
 RMS_EPS = 1e-06
+
+
+def press_the_scales(slab_in, mesh_name="sp"):
+    fan = lax.axis_size(mesh_name)
+    block_next = slab_in
+    right_arr = [(q - 1, q) for q in range(1, fan)] + [(fan - 1, 0)]
+    nodes = [block_next]
+    for _ in range(fan - 1):
+        block_next = lax.ppermute(block_next, mesh_name, perm=right_arr)
+        nodes += [block_next]
+    return jnp.roll(
+        jnp.concatenate([*reversed(nodes)], 0),
+        (lax.axis_index(mesh_name) + 1) * block_next.shape[0],
+        0,
+    )
 
 
 def shifted(value, axis, by):
@@ -195,7 +210,7 @@
     half_sum = chip_sum.astype(jnp.float32) + swapped(chip_sum, "tp", 2).astype(jnp.float32)
     resid_half = lax.dynamic_slice_in_dim(resid, core * half_width, half_width, 1)
     mid_half = (resid_half.astype(jnp.float32) + half_sum).astype(jnp.bfloat16)
-    mid_all = lax.all_gather(mid_half, "sp", axis=0, tiled=True)
+    mid_all = press_the_scales(mid_half)
     mid_peer = swapped(mid_half, "tp", 1)
     first = jnp.where(core == 0, mid_half, mid_peer)
     second = jnp.where(core == 0, mid_peer, mid_half)

time: 231 us -> 251 us (1.087)
  waiting for transfers between devices: 123 us -> 137 us
  local copies, waits for them, and re-layouts: 5.9 us -> 12.6 us
    ppermute x0 -> x7, waiting for transfers between devices: none -> 65.6 us  [press_the_scales(): block_next = lax.ppermute(block_next, mesh_name, perm=right_arr)]
    all_gather x1 -> x0, waiting for transfers between devices: 50.1 us -> none  [body_dense(): mid_all = lax.all_gather(mid_half, 'sp', axis=0, tiled=True)]
    unnamed x24 -> x44, local copies, waits for them, and re-layouts: 1.23 us -> 4.9 us
    ppermute x7, waiting for transfers between devices: 14.8 us -> 12.3 us  [swapped(): return lax.ppermute(value, axis, [(i, i ^ bit) for i in range(size)])]
  transfers between devices with their start and end apart: 10 -> 16, of which waited for: 7 -> 12; matrix products, arithmetic and copies ran while one was open for 10% -> 10% of each run, Pallas kernels for 0% -> 0%
where the time goes in v1:
time: 251 us
  waiting for transfers between devices  137 us (55%)
  blocking collectives  42.6 us (17%)
  matrix products  24.8 us (10%)
  between operations  13.8 us (5%)
  local copies, waits for them, and re-layouts  12.6 us (5%)
  starting transfers between devices  10.4 us (4%)
  other arithmetic  9.96 us (4%)
    ppermute x7, waiting for transfers between devices, press_the_scales(): block_next = lax.ppermute(block_next, mesh_name, perm=right_arr)  65.6 us
    reduce_scatter x1, waiting for transfers between devices, body_dense(): summed = lax.psum_scatter(both, 'sp', scatter_dimension=0, tiled=True)  58.9 us
    all_gather x1, blocking collectives, body_dense(): weight_all = lax.all_gather(weight_mat, 'sp', axis=0, tiled=True)  30.8 us
    ppermute x7, waiting for transfers between devices, swapped(): return lax.ppermute(value, axis, [(i, i ^ bit) for i in range(size)])  12.3 us
    dot_general x1, matrix products, body_dense(): up_part = jnp.dot(rows, exp_up[0], preferred_element_type=jnp.float32)  6.37 us
    psum x1, blocking collectives, body_dense(): lax.psum((jnp.sum(conv_out, axis=1), jnp.sum(conv_out * conv_out, axis=1)...  6.33 us
    all_gather x1, blocking collectives, body_dense(): lax.all_gather(shared_hidden, 'tp', axis=1, tiled=True)  5.45 us
  transfers between devices with their start and end apart: 16, of which 12 were waited for; matrix products, arithmetic and copies ran while one was open for 10% of the time, Pallas kernels for 0%

profile of v1, /device:TPU:0, one launch (start us, length us, event | category | flops | bytes accessed | tf_op | source)
XLA Modules:
  0.0 250.9 jit_solution(8320756707108558402)
XLA Ops:
  6.5 1.0 multiply_convert_fusion.4
  7.6 4.9 %collective-permute-start = (bf16[30,256]{1,0:T(8,128)(2,1)S(1)}, bf16[30,256]{1,0:T(8,128)(2,1)S(1)}, u32[]{:S(2)}, u32[]{:S(2)}) collective-permute-start(bf16[30,256]{1,0:T(8,128)(2,1)S(1)} %slice.261), channel_id=1, source_target_pairs={{0,4},{4,8},{8,12},{12,16},{16,20},{20,24},{24,28},{1,5},{5,9},{9,... | collective-permute-start | bytes 46088 | tf_op jit(solution)/shard_map/ppermute | solution.py:28
  12.4 1.0 fusion.73
  13.5 1.0 fusion.74
  14.5 1.3 fusion.71
  15.8 6.3 %all-reduce = (f32[128]{0:T(128)S(1)}, f32[128]{0:T(128)S(1)}) all-reduce(f32[128]{0:T(128)S(1)} %get-tuple-element.6, f32[128]{0:T(128)S(1)} %get-tuple-element.5), channel_id=1, replica_groups=mesh['sp'=8,'tp'=4] {'tp'}, use_global_device_ids=true, to_apply=%region_3.4 | all-reduce | flops 256 | bytes 2048 | tf_op jit(solution)/shard_map/psum | solution.py:198
  22.2 0.4 fusion.51
  22.7 1.5 collective-permute-done.1
  24.3 1.1 collective-permute-start.2
  25.4 7.3 %collective-permute-done.2 = bf16[128,1024]{1,0:T(8,128)(2,1)S(1)} collective-permute-done((bf16[128,1024]{1,0:T(8,128)(2,1)S(1)}, bf16[128,1024]{1,0:T(8,128)(2,1)S(1)}, u32[]{:S(2)}, u32[]{:S(2)}) %collective-permute-start.2) | collective-permute-done | bytes 262176 | tf_op jit(solution)/shard_map/ppermute | solution.py:145
  32.7 0.1 add_convert_fusion
  32.8 1.6 collective-permute-start.4
  34.5 8.6 %collective-permute-done.4 = bf16[128,1024]{1,0:T(8,128)(2,1)S(1)} collective-permute-done((bf16[128,1024]{1,0:T(8,128)(2,1)S(1)}, bf16[128,1024]{1,0:T(8,128)(2,1)S(1)}, u32[]{:S(2)}, u32[]{:S(2)}) %collective-permute-start.4) | collective-permute-done | bytes 262176 | tf_op jit(solution)/shard_map/ppermute | solution.py:16
  43.1 9.3 %collective-permute-done.5 = bf16[128,1024]{1,0:T(8,128)(2,1)S(1)} collective-permute-done((bf16[128,1024]{1,0:T(8,128)(2,1)S(1)}, bf16[128,1024]{1,0:T(8,128)(2,1)S(1)}, u32[]{:S(2)}, u32[]{:S(2)}) %collective-permute-start.5) | collective-permute-done | bytes 262176 | tf_op jit(solution)/shard_map/ppermute | solution.py:16
  52.4 9.1 %collective-permute-done.6 = bf16[128,1024]{1,0:T(8,128)(2,1)S(1)} collective-permute-done((bf16[128,1024]{1,0:T(8,128)(2,1)S(1)}, bf16[128,1024]{1,0:T(8,128)(2,1)S(1)}, u32[]{:S(2)}, u32[]{:S(2)}) %collective-permute-start.6) | collective-permute-done | bytes 262176 | tf_op jit(solution)/shard_map/ppermute | solution.py:16
  61.5 9.1 %collective-permute-done.7 = bf16[128,1024]{1,0:T(8,128)(2,1)S(1)} collective-permute-done((bf16[128,1024]{1,0:T(8,128)(2,1)S(1)}, bf16[128,1024]{1,0:T(8,128)(2,1)S(1)}, u32[]{:S(2)}, u32[]{:S(2)}) %collective-permute-start.7) | collective-permute-done | bytes 262176 | tf_op jit(solution)/shard_map/ppermute | solution.py:16
  70.6 9.7 %collective-permute-done.8 = bf16[128,1024]{1,0:T(8,128)(2,1)S(1)} collective-permute-done((bf16[128,1024]{1,0:T(8,128)(2,1)S(1)}, bf16[128,1024]{1,0:T(8,128)(2,1)S(1)}, u32[]{:S(2)}, u32[]{:S(2)}) %collective-permute-start.8) | collective-permute-done | bytes 262176 | tf_op jit(solution)/shard_map/ppermute | solution.py:16
  80.2 10.8 %collective-permute-done.9 = bf16[128,1024]{1,0:T(8,128)(2,1)S(1)} collective-permute-done((bf16[128,1024]{1,0:T(8,128)(2,1)S(1)}, bf16[128,1024]{1,0:T(8,128)(2,1)S(1)}, u32[]{:S(2)}, u32[]{:S(2)}) %collective-permute-start.9) | collective-permute-done | bytes 262176 | tf_op jit(solution)/shard_map/ppermute | solution.py:16
  91.0 9.1 %collective-permute-done.10 = bf16[128,1024]{1,0:T(8,128)(2,1)S(1)} collective-permute-done((bf16[128,1024]{1,0:T(8,128)(2,1)S(1)}, bf16[128,1024]{1,0:T(8,128)(2,1)S(1)}, u32[]{:S(2)}, u32[]{:S(2)}) %collective-permute-start.10) | collective-permute-done | bytes 262176 | tf_op jit(solution)/shard_map/ppermute | solution.py:16
  100.3 0.5 copy-done.3
  100.9 1.0 constant_dynamic-update-slice_fusion.7
  102.1 1.9 copy-done.1
  104.0 1.5 constant_dynamic-slice_fusion.1
  105.5 3.2 %dynamic-slice_bitcast_fusion = bf16[2048,512]{1,0:T(8,128)(2,1)} fusion(bf16[1,4096,512]{2,1,0:T(8,128)(2,1)} %param.30, s32[]{:T(128)S(6)} %select_n.92), kind=kLoop, calls=%fused_computation.13 | loop fusion | bytes 4194308 | tf_op jit(solution)/shard_map/dynamic_slice | solution.py:178
  108.8 1.0 collective-permute-start.13
  109.8 0.2 collective-permute-done.11
  110.0 2.8 %broadcast_select_fusion.1 = (bf16[1024,1024]{1,0:T(8,128)(2,1)S(1)}, bf16[1024,1024]{1,0:T(8,128)(2,1)S(1)}) fusion(bf16[1024,1024]{1,0:T(8,128)(2,1)} %collective-permute-done.11, pred[]{:T(512)S(6)} %eq.13, bf16[2048,1024]{1,0:T(8,128)(2,1)S(1)} %copy-done.2, s32[]{:T(128)S(6)} %select_n.84), kind=kLoop, calls=%fused_computation.16 | loop fusion | flops 2097152 | bytes 8388613 | tf_op jit(solution)/shard_map/jit(_where)/select_n | solution.py:231
  112.9 1.0 fusion
  113.9 1.2 copy-done.10
  115.1 4.6 %fusion.5 = f32[1024,1024]{1,0:T(8,128)S(1)} fusion(bf16[1,2048,1024]{2,1,0:T(8,128)(2,1)S(1)} %copy-done.10, f32[2048]{0:T(1024)S(1)} %copy-done.14, f32[1024]{0:T(1024)S(1)} %add_rsqrt_fusion, bf16[1024,1024]{1,0:T(8,128)(2,1)S(1)} %get-tuple-element.11, bf16[1024,1024]{1,0:T(8,128)(2,1)S(1)} %get-tuple-element.10), kind=kOutput, calls=%fused_computation.8 | convolution fusion | flops 4309647360 | bytes 12595200 | tf_op jit(solution)/shard_map/dot_general | solution.py:236
  119.7 6.4 %multiply_convert_fusion = bf16[1024,1024]{1,0:T(8,128)(2,1)} fusion(f32[1024,1024]{1,0:T(8,128)S(1)} %fusion.5, bf16[1,2048,1024]{2,1,0:T(8,128)(2,1)S(1)} %copy-done.11, f32[2048]{0:T(1024)S(1)} %copy-done.14, f32[1024]{0:T(1024)S(1)} %add_rsqrt_fusion, bf16[1024,1024]{1,0:T(8,128)(2,1)S(1)} %get-tuple-element.11, ...), kind=kOutput, calls=%fused_computation.10 | convolution fusion | flops 4315938816 | bytes 14692352 | tf_op jit(solution)/shard_map/dot_general | solution.py:237
  126.1 0.1 collective-permute-start.12
  126.2 30.8 %all_gather.7 = f32[1024,8]{0,1:T(8,128)S(1)} all-gather(f32[128,8]{0,1:T(8,128)S(1)} %select_reduce_fusion), channel_id=1, replica_groups=mesh['sp'=8,'tp'=4] {'sp'}, dimensions={0}, use_global_device_ids=true | all-gather | bytes 36864 | tf_op jit(solution)/shard_map/all_gather | solution.py:191
  157.0 3.1 %fusion.12 = f32[1024,512]{1,0:T(8,128)S(1)} fusion(bf16[1024,1024]{1,0:T(8,128)(2,1)} %multiply_convert_fusion, bf16[1,4096,512]{2,1,0:T(8,128)(2,1)} %param.30, s32[]{:T(128)S(6)} %select_n.87), kind=kOutput, calls=%fused_computation.25 | convolution fusion | flops 1073741824 | bytes 5242884 | tf_op jit(solution)/shard_map/dot_general | solution.py:243
  160.2 3.1 %fusion.14 = f32[1024,512]{1,0:T(8,128)S(1)} fusion(bf16[1024,1024]{1,0:T(8,128)(2,1)} %collective-permute-done.12, bf16[2048,512]{1,0:T(8,128)(2,1)} %collective-permute-done.13, s32[]{:T(128)S(6)} %select_n.78), kind=kOutput, calls=%fused_computation.27 | convolution fusion | flops 1073741824 | bytes 5242884 | tf_op jit(solution)/shard_map/dot_general | solution.py:252
  163.3 3.1 %multiply_convert_fusion.1 = bf16[1024,512]{1,0:T(8,128)(2,1)S(1)} fusion(f32[1024,512]{1,0:T(8,128)S(1)} %fusion.14, bf16[1024,1024]{1,0:T(8,128)(2,1)} %multiply_convert_fusion, bf16[2048,512]{1,0:T(8,128)(2,1)} %collective-permute-done.13, s32[]{:T(128)S(6)} %select_n.77, f32[1024]{0:T(1024)S(1)} %bitcast.88), kind=kOutput, calls=%fused_computation.12 | convolution fusion | flops 1075314688 | bytes 6295556 | tf_op jit(solution)/shard_map/dot_general | solution.py:248
  166.4 3.1 %multiply_convert_fusion.2 = bf16[1024,512]{1,0:T(8,128)(2,1)S(1)} fusion(f32[1024,512]{1,0:T(8,128)S(1)} %fusion.12, bf16[1024,1024]{1,0:T(8,128)(2,1)} %collective-permute-done.12, f32[1024]{0:T(1024)S(1)} %bitcast.89, bf16[1,4096,512]{2,1,0:T(8,128)(2,1)} %param.30, s32[]{:T(128)S(6)} %select_n.88), kind=kOutput, calls=%fused_computation.14 | convolution fusion | flops 1075314688 | bytes 6295556 | tf_op jit(solution)/shard_map/dot_general | solution.py:245
  169.5 1.6 pad_maximum_fusion.1
  171.2 0.2 fusion.8
  171.4 0.4 fusion.63
  171.8 0.4 fusion.7
  172.1 5.4 %all_gather.6 = bf16[128,512]{1,0:T(8,128)(2,1)S(1)} all-gather(bf16[128,128]{1,0:T(8,128)(2,1)S(1)} %fusion.7), channel_id=1, replica_groups=mesh['sp'=8,'tp'=4] {'tp'}, dimensions={1}, use_global_device_ids=true | all-gather | bytes 163840 | tf_op jit(solution)/shard_map/all_gather | solution.py:226
  177.6 58.9 %reduce-scatter.2.cloned.1.call-done = bf16[128,1024]{1,0:T(8,128)(2,1)} async-done(((bf16[1024,1024]{1,0:T(8,128)(2,1)}), bf16[128,1024]{1,0:T(8,128)(2,1)}) %reduce-scatter.2.cloned.1.call-update) | async-done | bytes 262160 | tf_op jit(solution)/shard_map/reduce_scatter | solution.py:260
  236.5 0.9 slice.324
  237.4 1.5 collective-permute-start.14
  238.9 0.2 fusion.75
  239.1 3.3 %collective-permute-done.14 = bf16[128,512]{1,0:T(8,128)(2,1)S(1)} collective-permute-done((bf16[128,512]{1,0:T(8,128)(2,1)S(1)}, bf16[128,512]{1,0:T(8,128)(2,1)S(1)}, u32[]{:S(2)}, u32[]{:S(2)}) %collective-permute-start.14) | collective-permute-done | bytes 131104 | tf_op jit(solution)/shard_map/ppermute | solution.py:145
  242.4 1.7 add_convert_fusion.2
  (66 shorter events, 0.7 us)
Async XLA Ops:
  6.5 15.7 %copy-start = (bf16[256,2048]{1,0:T(8,128)(2,1)S(1)}, bf16[256,2048]{1,0:T(8,128)(2,1)}, u32[]{:S(2)}) copy-start(bf16[256,2048]{1,0:T(8,128)(2,1)} %param.24) | copy-start | bytes 3145732
  6.5 15.7 %copy-start.8 = (f32[256]{0:T(256)S(1)}, f32[256]{0:T(256)}, u32[]{:S(2)}) copy-start(f32[256]{0:T(256)} %param.23) | copy-start | bytes 3076
  6.5 15.7 %copy-start.9 = (f32[256]{0:T(256)S(1)}, f32[256]{0:T(256)}, u32[]{:S(2)}) copy-start(f32[256]{0:T(256)} %param.22) | copy-start | bytes 3076
  6.5 229.9 %reduce-scatter.2.cloned.1.call-start = ((), (), s32[]{:S(2)}) async-start(), calls=%async_computation.1 | async-start | bytes 2359296 | tf_op jit(solution)/shard_map/reduce_scatter | solution.py:260
  7.6 6.9 %collective-permute-start = (bf16[30,256]{1,0:T(8,128)(2,1)S(1)}, bf16[30,256]{1,0:T(8,128)(2,1)S(1)}, u32[]{:S(2)}, u32[]{:S(2)}) collective-permute-start(bf16[30,256]{1,0:T(8,128)(2,1)S(1)} %slice.261), channel_id=1, source_target_pairs={{0,4},{4,8},{8,12},{12,16},{16,20},{20,24},{24,28},{1,5},{5,9},{9,... | collective-permute-start | bytes 46088 | tf_op jit(solution)/shard_map/ppermute | solution.py:28
  14.5 18.3 %copy-start.5 = (bf16[128,2048]{1,0:T(8,128)(2,1)S(1)}, bf16[128,2048]{1,0:T(8,128)(2,1)}, u32[]{:S(2)}) copy-start(bf16[128,2048]{1,0:T(8,128)(2,1)} %param.17) | copy-start | bytes 1572868
  22.6 1.6 collective-permute-start.1
  24.3 8.4 %collective-permute-start.2 = (bf16[128,1024]{1,0:T(8,128)(2,1)S(1)}, bf16[128,1024]{1,0:T(8,128)(2,1)S(1)}, u32[]{:S(2)}, u32[]{:S(2)}) collective-permute-start(bf16[128,1024]{1,0:T(8,128)(2,1)S(1)} %add_convert_fusion.1), channel_id=1, source_target_pairs={{0,2},{1,3},{2,0},{3,1},{4,6},{5,7},{6,4},{7,5},{8,10},{9,11},{10,... | collective-permute-start | bytes 786440 | tf_op jit(solution)/shard_map/ppermute | solution.py:145
  32.8 10.2 %collective-permute-start.4 = (bf16[128,1024]{1,0:T(8,128)(2,1)S(1)}, bf16[128,1024]{1,0:T(8,128)(2,1)S(1)}, u32[]{:S(2)}, u32[]{:S(2)}) collective-permute-start(bf16[128,1024]{1,0:T(8,128)(2,1)S(1)} %add_convert_fusion), channel_id=1, source_target_pairs={{0,4},{4,8},{8,12},{12,16},{16,20},{20,24},{24,28},{28,0},{1,5},{5... | collective-permute-start | bytes 786440 | tf_op jit(solution)/shard_map/ppermute | solution.py:16
  43.1 9.3 %collective-permute-start.5 = (bf16[128,1024]{1,0:T(8,128)(2,1)S(1)}, bf16[128,1024]{1,0:T(8,128)(2,1)S(1)}, u32[]{:S(2)}, u32[]{:S(2)}) collective-permute-start(bf16[128,1024]{1,0:T(8,128)(2,1)S(1)} %collective-permute-done.4), channel_id=1, source_target_pairs={{0,4},{4,8},{8,12},{12,16},{16,20},{20,24},{24,28},{28,0},{1,5},{5... | collective-permute-start | bytes 786440 | tf_op jit(solution)/shard_map/ppermute | solution.py:16
  52.4 9.1 %collective-permute-start.6 = (bf16[128,1024]{1,0:T(8,128)(2,1)S(1)}, bf16[128,1024]{1,0:T(8,128)(2,1)S(1)}, u32[]{:S(2)}, u32[]{:S(2)}) collective-permute-start(bf16[128,1024]{1,0:T(8,128)(2,1)S(1)} %collective-permute-done.5), channel_id=1, source_target_pairs={{0,4},{4,8},{8,12},{12,16},{16,20},{20,24},{24,28},{28,0},{1,5},{5... | collective-permute-start | bytes 786440 | tf_op jit(solution)/shard_map/ppermute | solution.py:16
  61.5 9.1 %collective-permute-start.7 = (bf16[128,1024]{1,0:T(8,128)(2,1)S(1)}, bf16[128,1024]{1,0:T(8,128)(2,1)S(1)}, u32[]{:S(2)}, u32[]{:S(2)}) collective-permute-start(bf16[128,1024]{1,0:T(8,128)(2,1)S(1)} %collective-permute-done.6), channel_id=1, source_target_pairs={{0,4},{4,8},{8,12},{12,16},{16,20},{20,24},{24,28},{28,0},{1,5},{5... | collective-permute-start | bytes 786440 | tf_op jit(solution)/shard_map/ppermute | solution.py:16
  70.6 9.7 %collective-permute-start.8 = (bf16[128,1024]{1,0:T(8,128)(2,1)S(1)}, bf16[128,1024]{1,0:T(8,128)(2,1)S(1)}, u32[]{:S(2)}, u32[]{:S(2)}) collective-permute-start(bf16[128,1024]{1,0:T(8,128)(2,1)S(1)} %collective-permute-done.7), channel_id=1, source_target_pairs={{0,4},{4,8},{8,12},{12,16},{16,20},{20,24},{24,28},{28,0},{1,5},{5... | collective-permute-start | bytes 786440 | tf_op jit(solution)/shard_map/ppermute | solution.py:16
  80.2 10.8 %collective-permute-start.9 = (bf16[128,1024]{1,0:T(8,128)(2,1)S(1)}, bf16[128,1024]{1,0:T(8,128)(2,1)S(1)}, u32[]{:S(2)}, u32[]{:S(2)}) collective-permute-start(bf16[128,1024]{1,0:T(8,128)(2,1)S(1)} %collective-permute-done.8), channel_id=1, source_target_pairs={{0,4},{4,8},{8,12},{12,16},{16,20},{20,24},{24,28},{28,0},{1,5},{5... | collective-permute-start | bytes 786440 | tf_op jit(solution)/shard_map/ppermute | solution.py:16
  91.0 9.1 %collective-permute-start.10 = (bf16[128,1024]{1,0:T(8,128)(2,1)S(1)}, bf16[128,1024]{1,0:T(8,128)(2,1)S(1)}, u32[]{:S(2)}, u32[]{:S(2)}) collective-permute-start(bf16[128,1024]{1,0:T(8,128)(2,1)S(1)} %collective-permute-done.9), channel_id=1, source_target_pairs={{0,4},{4,8},{8,12},{12,16},{16,20},{20,24},{24,28},{28,0},{1,5},{5... | collective-permute-start | bytes 786440 | tf_op jit(solution)/shard_map/ppermute | solution.py:16
  91.0 9.8 %collective-permute-start.3 = (bf16[128,1024]{1,0:T(8,128)(2,1)S(1)}, bf16[128,1024]{1,0:T(8,128)(2,1)S(1)}, u32[]{:S(2)}, u32[]{:S(2)}) collective-permute-start(bf16[128,1024]{1,0:T(8,128)(2,1)S(1)} %add_convert_fusion), channel_id=1, source_target_pairs={{0,1},{1,0},{2,3},{3,2},{4,5},{5,4},{6,7},{7,6},{8,9},{9,8},{10,11... | collective-permute-start | bytes 786440 | tf_op jit(solution)/shard_map/ppermute | solution.py:145
  100.1 0.7 copy-start.3
  102.1 2.0 copy-start.1
  105.5 4.5 %collective-permute-start.11 = (bf16[1024,1024]{1,0:T(8,128)(2,1)}, bf16[1024,1024]{1,0:T(8,128)(2,1)}, u32[]{:S(2)}, u32[]{:S(2)}) collective-permute-start(bf16[1024,1024]{1,0:T(8,128)(2,1)} %constant_dynamic-slice_fusion.1), channel_id=1, source_target_pairs={{0,1},{1,0},{2,3},{3,2},{4,5},{5,4},{6,7},{7,6},{8,9},{9,8},{10,11... | collective-permute-start | bytes 6291464 | tf_op jit(solution)/shard_map/ppermute | solution.py:145
  105.5 4.5 %copy-start.2 = (bf16[2048,1024]{1,0:T(8,128)(2,1)S(1)}, bf16[2048,1024]{1,0:T(8,128)(2,1)}, u32[]{:S(2)}) copy-start(bf16[2048,1024]{1,0:T(8,128)(2,1)} %copy-done.1) | copy-start | bytes 12582916
  108.8 51.3 %collective-permute-start.13 = (bf16[2048,512]{1,0:T(8,128)(2,1)}, bf16[2048,512]{1,0:T(8,128)(2,1)}, u32[]{:S(2)}, u32[]{:S(2)}) collective-permute-start(bf16[2048,512]{1,0:T(8,128)(2,1)} %dynamic-slice_bitcast_fusion), channel_id=1, source_target_pairs={{0,2},{1,3},{2,0},{3,1},{4,6},{5,7},{6,4},{7,5},{8,10},{9,11},{10,... | collective-permute-start | bytes 6291464 | tf_op jit(solution)/shard_map/ppermute | solution.py:145
  112.9 2.2 copy-start.10
  112.9 2.2 copy-start.14
  115.1 4.6 %copy-start.11 = (bf16[1,2048,1024]{2,1,0:T(8,128)(2,1)S(1)}, bf16[1,2048,1024]{2,1,0:T(8,128)(2,1)}, u32[]{:S(2)}) copy-start(bf16[1,2048,1024]{2,1,0:T(8,128)(2,1)} %param.29) | copy-start | bytes 12582916
  119.7 6.5 %copy-start.6 = (f32[128,4]{0,1:T(4,128)S(1)}, f32[128,4]{0,1:T(4,128)}, u32[]{:S(2)}) copy-start(f32[128,4]{0,1:T(4,128)} %param.27) | copy-start | bytes 6148
  119.7 6.5 %copy-start.7 = (s32[128,4]{0,1:T(4,128)S(1)}, s32[128,4]{0,1:T(4,128)}, u32[]{:S(2)}) copy-start(s32[128,4]{0,1:T(4,128)} %param.26) | copy-start | bytes 6148
  126.1 34.1 %collective-permute-start.12 = (bf16[1024,1024]{1,0:T(8,128)(2,1)}, bf16[1024,1024]{1,0:T(8,128)(2,1)}, u32[]{:S(2)}, u32[]{:S(2)}) collective-permute-start(bf16[1024,1024]{1,0:T(8,128)(2,1)} %multiply_convert_fusion), channel_id=1, source_target_pairs={{0,1},{1,0},{2,3},{3,2},{4,5},{5,4},{6,7},{7,6},{8,9},{9,8},{10,11... | collective-permute-start | bytes 6291464 | tf_op jit(solution)/shard_map/ppermute | solution.py:145
  169.5 1.9 copy-start.12
  169.5 2.2 copy-start.13
  171.2 67.8 %copy-start.4 = (bf16[512,512]{1,0:T(8,128)(2,1)S(1)}, bf16[512,512]{1,0:T(8,128)(2,1)}, u32[]{:S(2)}) copy-start(bf16[512,512]{1,0:T(8,128)(2,1)} %param.33) | copy-start | bytes 1572868
  237.4 5.0 %collective-permute-start.14 = (bf16[128,512]{1,0:T(8,128)(2,1)S(1)}, bf16[128,512]{1,0:T(8,128)(2,1)S(1)}, u32[]{:S(2)}, u32[]{:S(2)}) collective-permute-start(bf16[128,512]{1,0:T(8,128)(2,1)S(1)} %slice.324), channel_id=1, source_target_pairs={{0,2},{1,3},{2,0},{3,1},{4,6},{5,7},{6,4},{7,5},{8,10},{9,11},{10,... | collective-permute-start | bytes 393224 | tf_op jit(solution)/shard_map/ppermute | solution.py:145
Sparse Core Ops, SparseCore 0:
  171.3 65.1 reduce-scatter.1
